TPU v7x, 32 devices: a whole 2x2x4 slice. The times are simulated.
32 devices in a mesh: ep: 4 (over y, x), tp: 8 (over z, core).
Axes of the slice: x: 2, y: 2, z: 4, core: 2. Of those that a mesh axis runs over, the one named last changes fastest.
Arguments:
- tokens: bfloat16 [1024, 1024], P(('ep', 'tp')), may hold values from -6 to 6
- norm_gain: float32 [1024], replicated, may hold values from 0.5 to 1.5
- routing: int32 [1024, 2], P('ep'), may hold values from 0 to 7, as said below
- gate_share: float32 [1024, 2], P('ep'), may hold values from 0.5 to 1.5
- w_gate: bfloat16 [8, 1024, 256], P('ep', None, 'tp'), may hold values from -0.1875 to 0.1875
- w_up: bfloat16 [8, 1024, 256], P('ep', None, 'tp'), may hold values from -0.1875 to 0.1875
- w_down: bfloat16 [8, 256, 1024], P('ep', 'tp'), may hold values from -0.375 to 0.375
Outputs:
- mixed_out: bfloat16 [1024, 1024], P('ep', 'tp')
Inputs may be any that keep to these rules, and one draw needn't show every extreme that they name: `routing`: each row names two different experts whose ids lie in the same block of 2 consecutive ids. In each aligned block of 256 rows (the tokens of one index of ep) no expert is named by more than 128 rows, and some expert is named by exactly 128.
All inputs are finite; a program needn't handle non-finite values.
Results may differ from a plain program's by a relative error of at most 0.0015.
Values may be sent and summed in bfloat16 or wider, within the bound.
A program may use at most 64 MiB of HBM per device.

v0:
```python
import jax
import jax.numpy as jnp
from jax import lax
from jax.sharding import PartitionSpec as P

epsilon = 1e-06


def norm_rows(tokens, norm_gain):
    as_float = tokens.astype(jnp.float32)
    scaled = as_float * lax.rsqrt(jnp.mean(as_float * as_float, axis=-1, keepdims=True) + epsilon)
    return (scaled * norm_gain.astype(jnp.float32)).astype(jnp.bfloat16)


def fill_buffer(group, flat_target, slots, model_width):
    buffer = jnp.zeros((slots, model_width), jnp.bfloat16)
    return buffer.at[flat_target].set(jnp.repeat(group, 2, axis=0))


def body(tokens, norm_gain, routing, gate_share, w_gate, w_up, w_down):
    ep_size = lax.axis_size("ep")
    tp_size = lax.axis_size("tp")
    local_experts = w_gate.shape[0]
    experts = local_experts * ep_size
    group_rows = routing.shape[0]
    capacity = group_rows * 4 // experts
    model_width = tokens.shape[1]
    columns = model_width // tp_size
    normed = norm_rows(tokens, norm_gain)
    onehot = (routing[:, :, None] == jnp.arange(experts, dtype=jnp.int32)[None, None, :]).astype(
        jnp.int32
    )
    flat_hot = onehot.reshape(group_rows * 2, experts)
    ranking = jnp.cumsum(flat_hot, axis=0) - 1
    slot_pos = jnp.sum(ranking * flat_hot, axis=1).reshape(group_rows, 2)
    target = (routing * capacity + slot_pos).astype(jnp.int32)
    flat_target = target.reshape(-1)
    slice_len = capacity // tp_size
    tp_index = lax.axis_index("tp")
    group = lax.all_gather(normed, "tp", axis=0, tiled=True)
    buffer = fill_buffer(group, flat_target, experts * capacity, model_width)
    shaped = buffer.reshape(ep_size, local_experts, capacity, model_width)
    mine = lax.dynamic_slice_in_dim(shaped, tp_index * slice_len, slice_len, 2)
    mine = mine.reshape(ep_size, local_experts * slice_len, model_width)
    landed = lax.all_to_all(mine, "ep", split_axis=0, concat_axis=0, tiled=True)
    landed = landed.reshape(ep_size, local_experts, slice_len, model_width).transpose(1, 0, 2, 3)
    landed = landed.reshape(local_experts, ep_size * slice_len, model_width)
    full_gate, full_up, full_down = (
        lax.all_gather(w_gate, "tp", axis=2, tiled=True),
        lax.all_gather(w_up, "tp", axis=2, tiled=True),
        lax.all_gather(w_down, "tp", axis=1, tiled=True),
    )
    gate_sum = jnp.einsum("erd,edh->erh", landed, full_gate, preferred_element_type=jnp.float32)
    up_sum = jnp.einsum("erd,edh->erh", landed, full_up, preferred_element_type=jnp.float32)
    hidden = (jax.nn.silu(gate_sum) * up_sum).astype(jnp.bfloat16)
    produced = jnp.einsum(
        "erh,ehd->erd", hidden, full_down, preferred_element_type=jnp.float32
    ).astype(jnp.bfloat16)
    produced = produced.reshape(local_experts, ep_size, slice_len, model_width)
    blocks = lax.all_to_all(produced, "tp", split_axis=3, concat_axis=2, tiled=True)
    leaving = blocks.transpose(1, 0, 2, 3).reshape(ep_size, local_experts * capacity, columns)
    returned = lax.all_to_all(leaving, "ep", split_axis=0, concat_axis=0, tiled=True).reshape(
        experts * capacity, columns
    )
    picked_out = returned[target]
    mixed_out = jnp.sum(gate_share[:, :, None] * picked_out.astype(jnp.float32), axis=1)
    return mixed_out.astype(jnp.bfloat16)


def solution(mesh):
    return jax.shard_map(
        body,
        mesh=mesh,
        in_specs=(
            P(("ep", "tp"), None),
            P(),
            P("ep", None),
            P("ep", None),
            P("ep", None, "tp"),
            P("ep", None, "tp"),
            P("ep", "tp", None),
        ),
        out_specs=P("ep", "tp"),
        check_vma=False,
    )
```

profile of v0, /device:TPU:0, one launch (start us, length us, event | category | flops | bytes accessed | tf_op | source)
XLA Modules:
  0.0 124.2 jit_solution(3098279486913121579)
XLA Ops:
  6.5 0.0 all-gather.4.cloned.1.call-start
  6.5 0.7 all-gather.4.cloned.1.call-update
  7.3 0.0 all-gather.6.cloned.1.call-start
  7.3 0.7 all-gather.6.cloned.1.call-update
  8.0 0.0 all-gather.8.cloned.1.call-start
  8.1 0.7 all-gather.8.cloned.1.call-update
  8.7 0.8 copy.34
  9.6 0.1 eq.30
  9.7 0.1 eq.26
  9.9 1.1 reduce-window.6
  11.0 0.2 slice_reduce_fusion
  11.3 0.1 fusion.13
  11.4 0.1 reshape.89
  11.5 0.1 copy.36
  11.6 0.7 compare_select_fusion.1
  12.3 0.1 copy.37
  12.4 0.2 reshape.90
  12.6 1.0 fusion.4
  13.6 0.9 fusion.6
  14.5 19.1 %all_gather.12 = bf16[256,1024]{1,0:T(8,128)(2,1)S(1)} all-gather(bf16[32,1024]{1,0:T(8,128)(2,1)S(1)} %fusion.6), channel_id=1, replica_groups=mesh['ep'=4,'tp'=8] {'tp'}, dimensions={0}, use_global_device_ids=true | all-gather | bytes 589824 | tf_op jit(solution)/shard_map/all_gather | solution.py:40
  33.6 0.5 broadcast_in_dim.7
  34.2 0.4 reshape.111
  34.6 3.2 %scatter_custom_fusion = bf16[1024,1024]{1,0:T(8,128)(2,1)S(1)} fusion(s32[512]{0:T(512)S(1)} %bitcast.42, bf16[512,1024]{1,0:T(8,128)(2,1)S(1)} %reshape.111, bf16[]{:T(256)} %constant.11.clone.1), kind=kCustom, calls=%fused_computation.5 | custom fusion | bytes 2097154 | tf_op jit(solution)/shard_map/scatter | solution.py:17
  37.9 9.8 %all_to_all.28 = bf16[4,32,1024]{2,1,0:T(8,128)(2,1)S(1)} all-to-all(bf16[4,32,1024]{2,1,0:T(8,128)(2,1)S(1)} %bitcast.38), channel_id=1, replica_groups=mesh['ep'=4,'tp'=8] {'ep'}, dimensions={0} | all-to-all | bytes 524288 | tf_op jit(solution)/shard_map/all_to_all | solution.py:45
  47.7 0.0 all-gather.4.cloned.1.call-done
  47.7 1.7 %fusion.16 = f32[2,64,256]{2,1,0:T(8,128)S(1)} fusion(bf16[2,64,1024]{2,1,0:T(8,128)(2,1)S(1)} %bitcast.36, bf16[2,1024,256]{1,2,0:T(8,128)(2,1)} %all-gather.4.cloned.1.call-done), kind=kOutput, calls=%fused_computation.33 | convolution fusion | flops 67108864 | bytes 1441792 | tf_op jit(solution)/shard_map/erd,edh->erh/dot_general | solution.py:53
  49.4 10.8 %all-gather.6.cloned.1.call-done = bf16[2,1024,256]{1,2,0:T(8,128)(2,1)} async-done(((bf16[2,1024,32]{1,2,0:T(8,128)(2,1)}), bf16[2,1024,256]{1,2,0:T(8,128)(2,1)}) %all-gather.6.cloned.1.call-update) | async-done | bytes 1048592 | tf_op jit(solution)/shard_map/all_gather | solution.py:50
  60.2 23.5 %all-gather.8.cloned.1.call-done = bf16[2,256,1024]{2,1,0:T(8,128)(2,1)} async-done(((bf16[2,32,1024]{2,1,0:T(8,128)(2,1)}), bf16[2,256,1024]{2,1,0:T(8,128)(2,1)}) %all-gather.8.cloned.1.call-update) | async-done | bytes 1048592 | tf_op jit(solution)/shard_map/all_gather | solution.py:51
  83.7 2.2 %convolution_convert_fusion = bf16[2,64,1024]{2,1,0:T(8,128)(2,1)S(1)} fusion(bf16[2,256,1024]{2,1,0:T(8,128)(2,1)} %all-gather.8.cloned.1.call-done, bf16[2,64,1024]{2,1,0:T(8,128)(2,1)S(1)} %bitcast.37, bf16[2,1024,256]{1,2,0:T(8,128)(2,1)} %all-gather.6.cloned.1.call-done, f32[2,64,256]{2,1,0:T(8,128)S(1)} %fusion.16), kind=kOutput, calls=%fused_computation.2 | convolution fusion | flops 134545408 | bytes 2752512 | tf_op jit(solution)/shard_map/erh,ehd->erd/dot_general | solution.py:56
  85.9 1.4 %copy.39 = bf16[2,4,16,1024]{2,1,0,3:T(4,128)(2,1)S(1)} copy(bf16[2,4,16,1024]{3,2,1,0:T(8,128)(2,1)S(1)} %bitcast.40) | data formatting | bytes 524288 | tf_op jit(solution)/shard_map/reshape | solution.py:59
  87.3 2.2 %reshape.121 = bf16[8,2,8192]{2,1,0:T(2,128)(2,1)S(1)} reshape(bf16[1024,2,4,16]{3,2,1,0:T(4,128)(2,1)S(1)} %bitcast.32) | data formatting | bytes 524288
  89.5 12.9 %all_to_all.29 = bf16[8,2,8192]{2,1,0:T(2,128)(2,1)S(1)} all-to-all(bf16[8,2,8192]{2,1,0:T(2,128)(2,1)S(1)} %reshape.121), channel_id=1, replica_groups=mesh['ep'=4,'tp'=8] {'tp'}, dimensions={0} | all-to-all | bytes 524288 | tf_op jit(solution)/shard_map/all_to_all | solution.py:60
  102.3 1.4 %reshape.122 = bf16[1024,2,4,16]{3,2,1,0:T(4,128)(2,1)S(1)} reshape(bf16[8,2,8192]{2,1,0:T(2,128)(2,1)S(1)} %all_to_all.29) | data formatting | bytes 524288
  103.8 0.0 copy-start
  103.8 2.6 %copy.46 = bf16[2,4,16,8,128]{4,2,3,0,1:T(8,128)(2,1)} copy(bf16[2,4,16,8,128]{2,1,0,4,3:T(4,128)(2,1)S(1)} %bitcast.33) | data formatting | bytes 524288 | tf_op jit(solution)/shard_map/transpose | solution.py:61
  106.4 3.6 %all-to-all-start.2 = ((bf16[4,256,128]{2,1,0:T(8,128)(2,1)}), bf16[4,256,128]{2,1,0:T(8,128)(2,1)S(1)}, u32[]{:S(2)}, u32[]{:S(2)}) async-start(bf16[4,256,128]{2,1,0:T(8,128)(2,1)} %bitcast.15), calls=%async_computation.2 | async-start | bytes 524288 | tf_op jit(solution)/shard_map/all_to_all | solution.py:62
  109.9 0.1 copy.43
  110.1 0.1 reshape.101
  110.2 0.0 copy-done
  110.2 0.1 copy.33
  110.4 4.9 %all-to-all-done.2 = bf16[4,256,128]{2,1,0:T(8,128)(2,1)S(1)} async-done(((bf16[4,256,128]{2,1,0:T(8,128)(2,1)}), bf16[4,256,128]{2,1,0:T(8,128)(2,1)S(1)}, u32[]{:S(2)}, u32[]{:S(2)}) %all-to-all-start.2) | async-done | bytes 262176 | tf_op jit(solution)/shard_map/all_to_all | solution.py:62
  115.3 1.3 %gather_fusion = bf16[512,128]{1,0:T(8,128)(2,1)S(1)} fusion(bf16[1024,128]{1,0:T(8,128)(2,1)S(1)} %bitcast.34, s32[1024]{0:T(1024)S(1)} %pad_clamp_fusion), kind=kCustom, calls=%fused_computation | custom fusion | bytes 264192 | tf_op jit(solution)/shard_map/gather | solution.py:65
  116.7 1.1 fusion.3
  (8 shorter events, 0.1 us)
Async XLA Ops:
  6.5 41.2 %all-gather.4.cloned.1.call-start = ((), (), s32[]{:S(2)}) async-start(), calls=%async_computation.3 | async-start | bytes 1179648 | tf_op jit(solution)/shard_map/all_gather | solution.py:49
  7.3 52.9 %all-gather.6.cloned.1.call-start = ((), (), s32[]{:S(2)}) async-start(), calls=%async_computation.4 | async-start | bytes 1179648 | tf_op jit(solution)/shard_map/all_gather | solution.py:50
  8.0 75.7 %all-gather.8.cloned.1.call-start = ((), (), s32[]{:S(2)}) async-start(), calls=%async_computation.5 | async-start | bytes 1179648 | tf_op jit(solution)/shard_map/all_gather | solution.py:51
  103.8 6.5 %copy-start = (f32[256,2]{0,1:T(2,128)S(1)}, f32[256,2]{0,1:T(2,128)}, u32[]{:S(2)}) copy-start(f32[256,2]{0,1:T(2,128)} %param.10) | copy-start | bytes 6148
  106.4 9.0 %all-to-all-start.2 = ((bf16[4,256,128]{2,1,0:T(8,128)(2,1)}), bf16[4,256,128]{2,1,0:T(8,128)(2,1)S(1)}, u32[]{:S(2)}, u32[]{:S(2)}) async-start(bf16[4,256,128]{2,1,0:T(8,128)(2,1)} %bitcast.15), calls=%async_computation.2 | async-start | bytes 524288 | tf_op jit(solution)/shard_map/all_to_all | solution.py:62
Sparse Core Ops, SparseCore 0:
  8.9 27.6 all-gather.3
  38.3 21.8 all-gather.5
  61.8 21.8 all-gather.7
where the time goes:
time: 125 us; the launch traced here: 124 us
  blocking collectives  41.8 us (33%)
  waiting for transfers between devices  41.3 us (33%)
  local copies, waits for them, and re-layouts  15.3 us (12%)
  between operations  13.3 us (11%)
  other arithmetic  4.95 us (4%)
  matrix products  3.9 us (3%)
  starting transfers between devices  3.66 us (3%)
    all_gather x1, waiting for transfers between devices, body(): lax.all_gather(w_down, 'tp', axis=1, tiled=True)  23.5 us
    all_gather x1, blocking collectives, body(): group = lax.all_gather(normed, 'tp', axis=0, tiled=True)  19.1 us
    all_to_all x1, blocking collectives, body(): lax.all_to_all(produced, 'tp', split_axis=3, concat_axis=2, tiled=True)  12.9 us
    all_gather x1, waiting for transfers between devices, body(): lax.all_gather(w_up, 'tp', axis=2, tiled=True)  10.8 us
    all_to_all x1, blocking collectives, body(): landed = lax.all_to_all(mine, 'ep', split_axis=0, concat_axis=0, tiled=True)  9.78 us
    all_to_all x1, waiting for transfers between devices, body(): lax.all_to_all(leaving, 'ep', split_axis=0, concat_axis=0, tiled=True)  4.92 us
    unnamed x6, local copies, waits for them, and re-layouts  4.55 us
    all_to_all x1, starting transfers between devices, body(): lax.all_to_all(leaving, 'ep', split_axis=0, concat_axis=0, tiled=True)  3.58 us
  transfers between devices with their start and end apart: 4, of which 3 were waited for; matrix products, arithmetic and copies ran while one was open for 10% of the time, Pallas kernels for 0%

commit v1 on v0

--- a/solution.py
+++ b/solution.py
@@ -4,6 +4,17 @@
 from jax.sharding import PartitionSpec as P
 
 epsilon = 1e-06
+
+
+def in_blocks(shard, dim, size):
+    before, after = (shard.shape[:dim], shard.shape[dim + 1 :])
+    return jnp.moveaxis(shard.reshape(*before, size, -1, *after), dim, 0)
+
+
+def laid_out(pieces, dim):
+    lengths = list(pieces.shape[1:])
+    lengths[dim] *= pieces.shape[0]
+    return jnp.moveaxis(pieces, 0, dim).reshape(lengths)
 
 
 def norm_rows(tokens, norm_gain):
@@ -57,7 +68,14 @@
         "erh,ehd->erd", hidden, full_down, preferred_element_type=jnp.float32
     ).astype(jnp.bfloat16)
     produced = produced.reshape(local_experts, ep_size, slice_len, model_width)
-    blocks = lax.all_to_all(produced, "tp", split_axis=3, concat_axis=2, tiled=True)
+    length, index = (lax.axis_size("tp"), lax.axis_index("tp"))
+    blocks_2 = in_blocks(produced, 3, length)
+    outs = [blocks_2[index]]
+    for turn in range(1, length):
+        sent = blocks_2[index ^ turn]
+        outs.append(lax.ppermute(sent, "tp", [(i, i ^ turn) for i in range(length)]))
+    blocks_2 = jnp.stack(outs)[index ^ jnp.arange(length)]
+    blocks = laid_out(blocks_2, 2)
     leaving = blocks.transpose(1, 0, 2, 3).reshape(ep_size, local_experts * capacity, columns)
     returned = lax.all_to_all(leaving, "ep", split_axis=0, concat_axis=0, tiled=True).reshape(
         experts * capacity, columns

time: 125 us -> 119 us (0.952)
  blocking collectives: 41.8 us -> 19.1 us
  starting transfers between devices: 3.66 us -> 15.7 us
  waiting for transfers between devices: 41.3 us -> 50.9 us
  local copies, waits for them, and re-layouts: 15.3 us -> 10.7 us
    all_to_all x2 -> x0, blocking collectives: 22.7 us -> none  [the longest x1 12.9 us: body(): lax.all_to_all(produced, 'tp', split_axis=3, concat_axis=2, tiled=True)]
    ppermute x0 -> x7, starting transfers between devices: none -> 8.39 us  [body(): lax.ppermute(sent, 'tp', [(i, i ^ turn) for i in range(length)])]
    all_to_all x0 -> x1, waiting for transfers between devices: none -> 5.86 us  [body(): landed = lax.all_to_all(mine, 'ep', split_axis=0, concat_axis=0, tiled=True)]
    ppermute x0 -> x7, waiting for transfers between devices: none -> 3.81 us  [body(): lax.ppermute(sent, 'tp', [(i, i ^ turn) for i in range(length)])]
    all_to_all x0 -> x1, starting transfers between devices: none -> 3.75 us  [body(): landed = lax.all_to_all(mine, 'ep', split_axis=0, concat_axis=0, tiled=True)]
    unnamed x6 -> x19, local copies, waits for them, and re-layouts: 4.55 us -> 1.11 us
    transpose x1, local copies, waits for them, and re-layouts: 2.57 us -> 0.71 us  [body(): blocks.transpose(1, 0, 2, 3)]
    reshape x1 -> x0, local copies, waits for them, and re-layouts: 1.36 us -> none  [body(): produced = produced.reshape(local_experts, ep_size, slice_len, model_width)]
  transfers between devices with their start and end apart: 4 -> 12, of which waited for: 3 -> 7; matrix products, arithmetic and copies ran while one was open for 10% -> 11% of each run, Pallas kernels for 0% -> 0%
where the time goes in v1:
time: 119 us
  waiting for transfers between devices  50.9 us (43%)
  blocking collectives  19.1 us (16%)
  starting transfers between devices  15.7 us (13%)
  between operations  13.3 us (11%)
  local copies, waits for them, and re-layouts  10.7 us (9%)
  other arithmetic  4.97 us (4%)
  matrix products  3.89 us (3%)
    all_gather x1, waiting for transfers between devices, body(): lax.all_gather(w_down, 'tp', axis=1, tiled=True)  23.5 us
    all_gather x1, blocking collectives, body(): group = lax.all_gather(normed, 'tp', axis=0, tiled=True)  19.1 us
    all_gather x1, waiting for transfers between devices, body(): lax.all_gather(w_up, 'tp', axis=2, tiled=True)  10.3 us
    ppermute x7, starting transfers between devices, body(): lax.ppermute(sent, 'tp', [(i, i ^ turn) for i in range(length)])  8.39 us
    all_to_all x1, waiting for transfers between devices, body(): landed = lax.all_to_all(mine, 'ep', split_axis=0, concat_axis=0, tiled=True)  5.86 us
    all_to_all x1, waiting for transfers between devices, body(): lax.all_to_all(leaving, 'ep', split_axis=0, concat_axis=0, tiled=True)  5.38 us
    ppermute x7, waiting for transfers between devices, body(): lax.ppermute(sent, 'tp', [(i, i ^ turn) for i in range(length)])  3.81 us
    all_to_all x1, starting transfers between devices, body(): landed = lax.all_to_all(mine, 'ep', split_axis=0, concat_axis=0, tiled=True)  3.75 us
  transfers between devices with their start and end apart: 12, of which 7 were waited for; matrix products, arithmetic and copies ran while one was open for 11% of the time, Pallas kernels for 0%

profile of v1, /device:TPU:0, one launch (start us, length us, event | category | flops | bytes accessed | tf_op | source)
XLA Modules:
  0.0 118.6 jit_solution(15147297797955810034)
XLA Ops:
  6.5 0.7 all-gather.4.cloned.1.call-update
  7.3 0.7 all-gather.6.cloned.1.call-update
  8.0 0.0 all-gather.8.cloned.1.call-start
  8.1 0.7 all-gather.8.cloned.1.call-update
  8.7 0.8 copy.41
  9.6 0.1 eq.30
  9.7 0.1 eq.26
  9.9 1.1 reduce-window.6
  11.0 0.2 slice_reduce_fusion
  11.3 0.1 fusion.14
  11.4 0.1 reshape.120
  11.5 0.1 copy.43
  11.6 0.7 compare_select_fusion.1
  12.3 0.1 copy.44
  12.4 0.1 reshape.121
  12.6 1.0 fusion.4
  13.6 0.9 fusion.6
  14.5 19.1 %all_gather.12 = bf16[256,1024]{1,0:T(8,128)(2,1)S(1)} all-gather(bf16[32,1024]{1,0:T(8,128)(2,1)S(1)} %fusion.6), channel_id=1, replica_groups=mesh['ep'=4,'tp'=8] {'tp'}, dimensions={0}, use_global_device_ids=true | all-gather | bytes 589824 | tf_op jit(solution)/shard_map/all_gather | solution.py:51
  33.6 0.5 broadcast_in_dim.7
  34.2 0.4 reshape.150
  34.6 3.2 %scatter_custom_fusion = bf16[1024,1024]{1,0:T(8,128)(2,1)S(1)} fusion(s32[512]{0:T(512)S(1)} %bitcast.88, bf16[512,1024]{1,0:T(8,128)(2,1)S(1)} %reshape.150, bf16[]{:T(256)} %constant.19.clone.1), kind=kCustom, calls=%fused_computation.6 | custom fusion | bytes 2097154 | tf_op jit(solution)/shard_map/scatter | solution.py:28
  37.9 0.7 constant_dynamic-slice_fusion.8
  38.6 3.8 %all-to-all-start = ((bf16[4,32,1024]{2,1,0:T(8,128)(2,1)}), bf16[4,32,1024]{2,1,0:T(8,128)(2,1)S(1)}, u32[]{:S(2)}, u32[]{:S(2)}) async-start(bf16[4,32,1024]{2,1,0:T(8,128)(2,1)} %bitcast.4), calls=%async_computation | async-start | bytes 524288 | tf_op jit(solution)/shard_map/all_to_all | solution.py:56
  42.4 5.9 %all-to-all-done = bf16[4,32,1024]{2,1,0:T(8,128)(2,1)S(1)} async-done(((bf16[4,32,1024]{2,1,0:T(8,128)(2,1)}), bf16[4,32,1024]{2,1,0:T(8,128)(2,1)S(1)}, u32[]{:S(2)}, u32[]{:S(2)}) %all-to-all-start) | async-done | bytes 262176 | tf_op jit(solution)/shard_map/all_to_all | solution.py:56
  48.3 1.7 %fusion.18 = f32[2,64,256]{2,1,0:T(8,128)S(1)} fusion(bf16[2,64,1024]{2,1,0:T(8,128)(2,1)S(1)} %bitcast.74, bf16[2,1024,256]{1,2,0:T(8,128)(2,1)} %all-gather.4.cloned.1.call-done), kind=kOutput, calls=%fused_computation.61 | convolution fusion | flops 67108864 | bytes 1441792 | tf_op jit(solution)/shard_map/erd,edh->erh/dot_general | solution.py:64
  49.9 10.3 %all-gather.6.cloned.1.call-done = bf16[2,1024,256]{1,2,0:T(8,128)(2,1)} async-done(((bf16[2,1024,32]{1,2,0:T(8,128)(2,1)}), bf16[2,1024,256]{1,2,0:T(8,128)(2,1)}) %all-gather.6.cloned.1.call-update) | async-done | bytes 1048592 | tf_op jit(solution)/shard_map/all_gather | solution.py:61
  60.2 23.5 %all-gather.8.cloned.1.call-done = bf16[2,256,1024]{2,1,0:T(8,128)(2,1)} async-done(((bf16[2,32,1024]{2,1,0:T(8,128)(2,1)}), bf16[2,256,1024]{2,1,0:T(8,128)(2,1)}) %all-gather.8.cloned.1.call-update) | async-done | bytes 1048592 | tf_op jit(solution)/shard_map/all_gather | solution.py:62
  83.7 2.2 %convolution_convert_fusion = bf16[2,64,1024]{2,1,0:T(8,128)(2,1)S(1)} fusion(bf16[2,256,1024]{2,1,0:T(8,128)(2,1)} %all-gather.8.cloned.1.call-done, bf16[2,64,1024]{2,1,0:T(8,128)(2,1)S(1)} %bitcast.75, bf16[2,1024,256]{1,2,0:T(8,128)(2,1)} %all-gather.6.cloned.1.call-done, f32[2,64,256]{2,1,0:T(8,128)S(1)} %fusion.18), kind=kOutput, calls=%fused_computation.3 | convolution fusion | flops 134545408 | bytes 2752512 | tf_op jit(solution)/shard_map/erh,ehd->erd/dot_general | solution.py:67
  86.0 0.6 constant_dynamic-slice_fusion
  86.6 0.3 collective-permute-start
  87.0 1.7 %collective-permute-start.1 = (bf16[2,4,16,128]{3,2,1,0:T(8,128)(2,1)S(1)}, bf16[2,4,16,128]{3,2,1,0:T(8,128)(2,1)S(1)}, u32[]{:S(2)}, u32[]{:S(2)}) collective-permute-start(bf16[2,4,16,128]{3,2,1,0:T(8,128)(2,1)S(1)} %bitcast.86), channel_id=1, source_target_pairs={{0,2},{1,3},{2,0},{3,1},{4,6},{5,7},{6,4},{7,5},{8,10},{9,11},{10,... | collective-permute-start | bytes 98312 | tf_op jit(solution)/shard_map/ppermute | solution.py:76
  88.6 0.1 collective-permute-start.2
  88.7 2.0 %collective-permute-start.3 = (bf16[2,4,16,128]{3,2,1,0:T(8,128)(2,1)S(1)}, bf16[2,4,16,128]{3,2,1,0:T(8,128)(2,1)S(1)}, u32[]{:S(2)}, u32[]{:S(2)}) collective-permute-start(bf16[2,4,16,128]{3,2,1,0:T(8,128)(2,1)S(1)} %bitcast.84), channel_id=1, source_target_pairs={{0,4},{1,5},{2,6},{3,7},{4,0},{5,1},{6,2},{7,3},{8,12},{9,13},{10,... | collective-permute-start | bytes 98312 | tf_op jit(solution)/shard_map/ppermute | solution.py:76
  90.7 0.8 collective-permute-start.4
  91.5 2.2 %collective-permute-start.5 = (bf16[2,4,16,128]{3,2,1,0:T(8,128)(2,1)S(1)}, bf16[2,4,16,128]{3,2,1,0:T(8,128)(2,1)S(1)}, u32[]{:S(2)}, u32[]{:S(2)}) collective-permute-start(bf16[2,4,16,128]{3,2,1,0:T(8,128)(2,1)S(1)} %bitcast.82), channel_id=1, source_target_pairs={{0,6},{1,7},{2,4},{3,5},{4,2},{5,3},{6,0},{7,1},{8,14},{9,15},{10,... | collective-permute-start | bytes 98312 | tf_op jit(solution)/shard_map/ppermute | solution.py:76
  93.6 1.5 %collective-permute-start.6 = (bf16[2,4,16,128]{3,2,1,0:T(8,128)(2,1)S(1)}, bf16[2,4,16,128]{3,2,1,0:T(8,128)(2,1)S(1)}, u32[]{:S(2)}, u32[]{:S(2)}) collective-permute-start(bf16[2,4,16,128]{3,2,1,0:T(8,128)(2,1)S(1)} %bitcast.81), channel_id=1, source_target_pairs={{0,7},{1,6},{2,5},{3,4},{4,3},{5,2},{6,1},{7,0},{8,15},{9,14},{10,... | collective-permute-start | bytes 98312 | tf_op jit(solution)/shard_map/ppermute | solution.py:76
  95.2 0.6 collective-permute-done.4
  95.8 1.5 %collective-permute-done.5 = bf16[2,4,16,128]{3,2,1,0:T(8,128)(2,1)S(1)} collective-permute-done((bf16[2,4,16,128]{3,2,1,0:T(8,128)(2,1)S(1)}, bf16[2,4,16,128]{3,2,1,0:T(8,128)(2,1)S(1)}, u32[]{:S(2)}, u32[]{:S(2)}) %collective-permute-start.5) | collective-permute-done | bytes 32800 | tf_op jit(solution)/shard_map/ppermute | solution.py:76
  97.3 1.7 %collective-permute-done.6 = bf16[2,4,16,128]{3,2,1,0:T(8,128)(2,1)S(1)} collective-permute-done((bf16[2,4,16,128]{3,2,1,0:T(8,128)(2,1)S(1)}, bf16[2,4,16,128]{3,2,1,0:T(8,128)(2,1)S(1)}, u32[]{:S(2)}, u32[]{:S(2)}) %collective-permute-start.6) | collective-permute-done | bytes 32800 | tf_op jit(solution)/shard_map/ppermute | solution.py:76
  99.0 0.6 gather_fusion
  99.6 0.7 copy.55
  100.3 3.5 %all-to-all-start.1 = ((bf16[4,256,128]{2,1,0:T(8,128)(2,1)}), bf16[4,256,128]{2,1,0:T(8,128)(2,1)S(1)}, u32[]{:S(2)}, u32[]{:S(2)}) async-start(bf16[4,256,128]{2,1,0:T(8,128)(2,1)} %bitcast.27), calls=%async_computation.1 | async-start | bytes 524288 | tf_op jit(solution)/shard_map/all_to_all | solution.py:80
  103.8 0.1 copy.56
  104.0 0.1 reshape.140
  104.1 0.1 copy.40
  104.3 5.4 %all-to-all-done.1 = bf16[4,256,128]{2,1,0:T(8,128)(2,1)S(1)} async-done(((bf16[4,256,128]{2,1,0:T(8,128)(2,1)}), bf16[4,256,128]{2,1,0:T(8,128)(2,1)S(1)}, u32[]{:S(2)}, u32[]{:S(2)}) %all-to-all-start.1) | async-done | bytes 262176 | tf_op jit(solution)/shard_map/all_to_all | solution.py:80
  109.6 1.3 %gather_fusion.1 = bf16[512,128]{1,0:T(8,128)(2,1)S(1)} fusion(bf16[1024,128]{1,0:T(8,128)(2,1)S(1)} %bitcast.71, s32[1024]{0:T(1024)S(1)} %pad_clamp_fusion), kind=kCustom, calls=%fused_computation.1 | custom fusion | bytes 264192 | tf_op jit(solution)/shard_map/gather | solution.py:83
  111.0 1.1 fusion.3
  (35 shorter events, 0.4 us)
Async XLA Ops:
  6.5 41.7 %all-gather.4.cloned.1.call-start = ((), (), s32[]{:S(2)}) async-start(), calls=%async_computation.2 | async-start | bytes 1179648 | tf_op jit(solution)/shard_map/all_gather | solution.py:60
  7.3 52.9 %all-gather.6.cloned.1.call-start = ((), (), s32[]{:S(2)}) async-start(), calls=%async_computation.3 | async-start | bytes 1179648 | tf_op jit(solution)/shard_map/all_gather | solution.py:61
  8.0 75.7 %all-gather.8.cloned.1.call-start = ((), (), s32[]{:S(2)}) async-start(), calls=%async_computation.4 | async-start | bytes 1179648 | tf_op jit(solution)/shard_map/all_gather | solution.py:62
  38.6 9.6 %all-to-all-start = ((bf16[4,32,1024]{2,1,0:T(8,128)(2,1)}), bf16[4,32,1024]{2,1,0:T(8,128)(2,1)S(1)}, u32[]{:S(2)}, u32[]{:S(2)}) async-start(bf16[4,32,1024]{2,1,0:T(8,128)(2,1)} %bitcast.4), calls=%async_computation | async-start | bytes 524288 | tf_op jit(solution)/shard_map/all_to_all | solution.py:56
  86.0 18.1 %copy-start = (f32[256,2]{0,1:T(2,128)S(1)}, f32[256,2]{0,1:T(2,128)}, u32[]{:S(2)}) copy-start(f32[256,2]{0,1:T(2,128)} %param.10) | copy-start | bytes 6148
  86.6 4.8 %collective-permute-start = (bf16[2,4,16,128]{3,2,1,0:T(8,128)(2,1)S(1)}, bf16[2,4,16,128]{3,2,1,0:T(8,128)(2,1)S(1)}, u32[]{:S(2)}, u32[]{:S(2)}) collective-permute-start(bf16[2,4,16,128]{3,2,1,0:T(8,128)(2,1)S(1)} %bitcast.87), channel_id=1, source_target_pairs={{0,1},{1,0},{2,3},{3,2},{4,5},{5,4},{6,7},{7,6},{8,9},{9,8},{10,11... | collective-permute-start | bytes 98312 | tf_op jit(solution)/shard_map/ppermute | solution.py:76
  87.0 6.7 %collective-permute-start.1 = (bf16[2,4,16,128]{3,2,1,0:T(8,128)(2,1)S(1)}, bf16[2,4,16,128]{3,2,1,0:T(8,128)(2,1)S(1)}, u32[]{:S(2)}, u32[]{:S(2)}) collective-permute-start(bf16[2,4,16,128]{3,2,1,0:T(8,128)(2,1)S(1)} %bitcast.86), channel_id=1, source_target_pairs={{0,2},{1,3},{2,0},{3,1},{4,6},{5,7},{6,4},{7,5},{8,10},{9,11},{10,... | collective-permute-start | bytes 98312 | tf_op jit(solution)/shard_map/ppermute | solution.py:76
  88.6 6.5 %collective-permute-start.2 = (bf16[2,4,16,128]{3,2,1,0:T(8,128)(2,1)S(1)}, bf16[2,4,16,128]{3,2,1,0:T(8,128)(2,1)S(1)}, u32[]{:S(2)}, u32[]{:S(2)}) collective-permute-start(bf16[2,4,16,128]{3,2,1,0:T(8,128)(2,1)S(1)} %bitcast.85), channel_id=1, source_target_pairs={{0,3},{1,2},{2,1},{3,0},{4,7},{5,6},{6,5},{7,4},{8,11},{9,10},{10,... | collective-permute-start | bytes 98312 | tf_op jit(solution)/shard_map/ppermute | solution.py:76
  88.7 6.4 %collective-permute-start.3 = (bf16[2,4,16,128]{3,2,1,0:T(8,128)(2,1)S(1)}, bf16[2,4,16,128]{3,2,1,0:T(8,128)(2,1)S(1)}, u32[]{:S(2)}, u32[]{:S(2)}) collective-permute-start(bf16[2,4,16,128]{3,2,1,0:T(8,128)(2,1)S(1)} %bitcast.84), channel_id=1, source_target_pairs={{0,4},{1,5},{2,6},{3,7},{4,0},{5,1},{6,2},{7,3},{8,12},{9,13},{10,... | collective-permute-start | bytes 98312 | tf_op jit(solution)/shard_map/ppermute | solution.py:76
  90.7 5.1 %collective-permute-start.4 = (bf16[2,4,16,128]{3,2,1,0:T(8,128)(2,1)S(1)}, bf16[2,4,16,128]{3,2,1,0:T(8,128)(2,1)S(1)}, u32[]{:S(2)}, u32[]{:S(2)}) collective-permute-start(bf16[2,4,16,128]{3,2,1,0:T(8,128)(2,1)S(1)} %bitcast.83), channel_id=1, source_target_pairs={{0,5},{1,4},{2,7},{3,6},{4,1},{5,0},{6,3},{7,2},{8,13},{9,12},{10,... | collective-permute-start | bytes 98312 | tf_op jit(solution)/shard_map/ppermute | solution.py:76
  91.5 5.8 %collective-permute-start.5 = (bf16[2,4,16,128]{3,2,1,0:T(8,128)(2,1)S(1)}, bf16[2,4,16,128]{3,2,1,0:T(8,128)(2,1)S(1)}, u32[]{:S(2)}, u32[]{:S(2)}) collective-permute-start(bf16[2,4,16,128]{3,2,1,0:T(8,128)(2,1)S(1)} %bitcast.82), channel_id=1, source_target_pairs={{0,6},{1,7},{2,4},{3,5},{4,2},{5,3},{6,0},{7,1},{8,14},{9,15},{10,... | collective-permute-start | bytes 98312 | tf_op jit(solution)/shard_map/ppermute | solution.py:76
  93.6 5.4 %collective-permute-start.6 = (bf16[2,4,16,128]{3,2,1,0:T(8,128)(2,1)S(1)}, bf16[2,4,16,128]{3,2,1,0:T(8,128)(2,1)S(1)}, u32[]{:S(2)}, u32[]{:S(2)}) collective-permute-start(bf16[2,4,16,128]{3,2,1,0:T(8,128)(2,1)S(1)} %bitcast.81), channel_id=1, source_target_pairs={{0,7},{1,6},{2,5},{3,4},{4,3},{5,2},{6,1},{7,0},{8,15},{9,14},{10,... | collective-permute-start | bytes 98312 | tf_op jit(solution)/shard_map/ppermute | solution.py:76
  100.3 9.3 %all-to-all-start.1 = ((bf16[4,256,128]{2,1,0:T(8,128)(2,1)}), bf16[4,256,128]{2,1,0:T(8,128)(2,1)S(1)}, u32[]{:S(2)}, u32[]{:S(2)}) async-start(bf16[4,256,128]{2,1,0:T(8,128)(2,1)} %bitcast.27), calls=%async_computation.1 | async-start | bytes 524288 | tf_op jit(solution)/shard_map/all_to_all | solution.py:80
Sparse Core Ops, SparseCore 0:
  8.9 27.6 all-gather.3
  38.3 21.8 all-gather.5
  61.8 21.8 all-gather.7
